TPU v7x, 32 devices: a whole 2x2x4 slice. The times are simulated.
32 devices in a mesh: fs: 4 (over z), rep: 4 (over y, x), tp: 2 (over core).
Axes of the slice: x: 2, y: 2, z: 4, core: 2. Of those that a mesh axis runs over, the one named last changes fastest.
Arguments:
- normed_input: bfloat16 [2048, 1024], P(('fs', 'rep')), may hold values from -6 to 6
- query_cotangent: bfloat16 [2048, 512], P(('fs', 'rep'), 'tp'), may hold values from -0.029907227 to 0.029907227
- value_cotangent: bfloat16 [2048, 1024], P(('fs', 'rep'), 'tp'), may hold values from -0.029907227 to 0.029907227
- query_basis: bfloat16 [1024, 128], replicated, may hold values from -0.1875 to 0.1875
- value_basis: bfloat16 [1024, 128], replicated, may hold values from -0.1875 to 0.1875
- query_weight: float32 [1024, 512], P(('fs', 'rep'), 'tp'), may hold values from -0.1875 to 0.1875
- value_weight: float32 [1024, 1024], P(('fs', 'rep'), 'tp'), may hold values from -0.1875 to 0.1875
- query_first: float32 [128, 512], P(('fs', 'rep'), 'tp'), may hold values from -6 to 6
- query_second: float32 [128, 512], P(('fs', 'rep'), 'tp'), may hold values from 0.25 to 4
- value_first: float32 [128, 1024], P(('fs', 'rep'), 'tp'), may hold values from -6 to 6
- value_second: float32 [128, 1024], P(('fs', 'rep'), 'tp'), may hold values from 0.25 to 4
Outputs:
- query_update: float32 [1024, 512], P(('fs', 'rep'), 'tp')
- value_update: float32 [1024, 1024], P(('fs', 'rep'), 'tp')
- query_weight_new: float32 [1024, 512], P(('fs', 'rep'), 'tp')
- value_weight_new: float32 [1024, 1024], P(('fs', 'rep'), 'tp')
- query_first_new: float32 [128, 512], P(('fs', 'rep'), 'tp')
- query_second_new: float32 [128, 512], P(('fs', 'rep'), 'tp')
- value_first_new: float32 [128, 1024], P(('fs', 'rep'), 'tp')
- value_second_new: float32 [128, 1024], P(('fs', 'rep'), 'tp')
- query_copy: bfloat16 [1024, 512], P(None, 'tp')
- value_copy: bfloat16 [1024, 1024], P(None, 'tp')
All inputs are finite; a program needn't handle non-finite values.
Results may differ from a plain program's by a relative error of at most 0.001.
Values may be sent and summed in bfloat16 or wider, within the bound.
A program may use at most 64 MiB of HBM per device.

v0:
```python
import functools
import jax
import jax.numpy as jnp
from jax import lax
from jax.experimental import pallas as pl
from jax.experimental.pallas import tpu as pltpu
from jax.sharding import PartitionSpec as P


def moments(projected, first_old, second_old):
    first_new = 0.9 * first_old + 0.1 * projected
    second_new = 0.99 * second_old + 0.01 * projected * projected
    return (first_new, second_new, first_new / (jnp.sqrt(second_new) + 1e-08))


def finish(whole_dir, basis_rows, weight, squares, entries):
    norm_scale = jnp.sqrt(squares / entries + 1.0)
    update = jnp.dot(basis_rows, whole_dir, precision=lax.Precision.HIGHEST) / norm_scale
    weight_new = weight - 0.01 * update
    return (update, weight_new, weight_new.astype(jnp.bfloat16))


def split_parts(reduced):
    high_part = reduced.astype(jnp.bfloat16)
    held = lax.optimization_barrier(high_part)
    low_part = (reduced - held.astype(jnp.float32)).astype(jnp.bfloat16)
    return (high_part, low_part)


def parts_product(high_part, low_part, cotangent):
    dims = (((0,), (0,)), ((), ()))
    first_term = lax.dot_general(high_part, cotangent, dims, preferred_element_type=jnp.float32)
    second_term = lax.dot_general(low_part, cotangent, dims, preferred_element_type=jnp.float32)
    return first_term + second_term


def body(
    normed_input,
    query_cotangent,
    value_cotangent,
    query_basis,
    value_basis,
    query_weight,
    value_weight,
    query_first,
    query_second,
    value_first,
    value_second,
):
    row_count = query_weight.shape[0]
    query_width = query_cotangent.shape[1]
    offset = lax.axis_index(("fs", "rep")) * row_count
    query_rows = lax.dynamic_slice_in_dim(query_basis, offset, row_count, 0).astype(jnp.float32)
    value_rows = lax.dynamic_slice_in_dim(value_basis, offset, row_count, 0).astype(jnp.float32)
    reduced_query = jnp.dot(normed_input, query_basis, preferred_element_type=jnp.float32)
    reduced_value = jnp.dot(normed_input, value_basis, preferred_element_type=jnp.float32)
    query_high, query_low = split_parts(reduced_query)
    value_high, value_low = split_parts(reduced_value)
    projected = lax.psum_scatter(
        jnp.concatenate(
            [
                parts_product(query_high, query_low, query_cotangent),
                parts_product(value_high, value_low, value_cotangent),
            ],
            axis=1,
        ),
        ("fs", "rep"),
        scatter_dimension=0,
        tiled=True,
    )
    query_projected = projected[:, :query_width]
    value_projected = projected[:, query_width:]
    query_first_new, query_second_new, query_dir = moments(
        query_projected, query_first, query_second
    )
    value_first_new, value_second_new, value_dir = moments(
        value_projected, value_first, value_second
    )
    query_whole, value_whole = (
        lax.all_gather(query_dir, ("fs", "rep"), axis=0, tiled=True),
        lax.all_gather(value_dir, ("fs", "rep"), axis=0, tiled=True),
    )
    query_squares, value_squares = lax.psum(
        (jnp.sum(query_dir * query_dir), jnp.sum(value_dir * value_dir)), ("fs", "rep", "tp")
    )
    tp_count = lax.axis_size("tp")
    query_update, query_weight_new, query_half = finish(
        query_whole,
        query_rows,
        query_weight,
        query_squares,
        query_whole.shape[0] * query_whole.shape[1] * tp_count,
    )
    value_update, value_weight_new, value_half = finish(
        value_whole,
        value_rows,
        value_weight,
        value_squares,
        value_whole.shape[0] * value_whole.shape[1] * tp_count,
    )
    query_copy, value_copy = (
        lax.all_gather(query_half, ("fs", "rep"), axis=0, tiled=True),
        lax.all_gather(value_half, ("fs", "rep"), axis=0, tiled=True),
    )
    return (
        query_update,
        value_update,
        query_weight_new,
        value_weight_new,
        query_first_new,
        query_second_new,
        value_first_new,
        value_second_new,
        query_copy,
        value_copy,
    )


MESH = pl.DeviceIdType.MESH
ORDER = (1, 3, 2)
EARLY_FS = 2
REP_AT = 1
SPLIT_EARLY = True
VMEM_LIMIT = 60 * 2**20
OUT_LIMIT = 16 * 2**20
f32, bf16 = jnp.float32, jnp.bfloat16


def two_parts(x):
    high = x.astype(bf16)
    return high, (x - high.astype(f32)).astype(bf16)


def three_parts(x):
    high = x.astype(bf16)
    rest = x - high.astype(f32)
    middle = rest.astype(bf16)
    return high, middle, (rest - middle.astype(f32)).astype(bf16)


def remote(src, dst, sems, index, peer):
    return pltpu.make_async_remote_copy(
        src_ref=src,
        dst_ref=dst,
        send_sem=sems[0].at[index],
        recv_sem=sems[1].at[index],
        device_id=peer,
        device_id_type=MESH,
    )


def kernel(
    F, R, T,
    x_hbm, qc_hbm, vc_hbm, qb_hbm, vb_hbm, qw_hbm, vw_hbm, qf_hbm, qs_hbm, vf_hbm, vs_hbm,
    u_ref, n_ref, fn_ref, sn_ref, copy_ref,
    x_ref, qc_ref, vc_ref, qb_ref, vb_ref, w_ref, f_ref, s_ref, near_ref,
    part, got1, mid, got2, dirs, squares, squares_in,
    load, s1, r1, s2, r2, s3, r3, s4, r4, s5, r5, s6, r6, s7, r7, s8, r8, s9, r9,
):
    z, r, t = lax.axis_index("fs"), lax.axis_index("rep"), lax.axis_index("tp")
    zs = [lax.rem(z + k, F) for k in range(F)]
    rs = [lax.rem(r + k, R) for k in range(R)]
    ts = [lax.rem(t + k, T) for k in range(T)]
    back = [lax.rem(z + F - k, F) for k in range(F)]
    if F == 4:
        pairs = {1: z + 1 - 2 * lax.rem(z, 2), 2: lax.rem(z + 2, 4), 3: 3 - z}
        zs = back = [z] + [pairs[k] for k in ORDER]
    rows = qw_hbm.shape[0]
    QC, VC = qc_hbm.shape[1], vc_hbm.shape[1]
    M = qf_hbm.shape[0]

    barrier = pltpu.get_barrier_semaphore()
    for axis, others in (("rep", rs), ("fs", zs), ("tp", ts)):
        for other in others[1:]:
            pl.semaphore_signal(barrier, inc=1, device_id={axis: other}, device_id_type=MESH)

    query, value = pl.ds(0, QC), pl.ds(QC, VC)
    loads = [
        pltpu.make_async_copy(src, dst, load.at[i])
        for i, (src, dst) in enumerate((
            (x_hbm, x_ref),
            (qb_hbm, qb_ref),
            (qc_hbm, qc_ref),
            (vb_hbm, vb_ref),
            (vc_hbm, vc_ref),
            (qf_hbm, f_ref.at[:, query]),
            (vf_hbm, f_ref.at[:, value]),
            (qs_hbm, s_ref.at[:, query]),
            (vs_hbm, s_ref.at[:, value]),
            (qw_hbm, w_ref.at[:, query]),
            (vw_hbm, w_ref.at[:, value]),
        ))
    ]
    for c in loads:
        c.start()

    loads[0].wait()
    x = x_ref[...]
    for i, (basis, cot, start, width) in enumerate(
        ((qb_ref, qc_ref, 0, QC), (vb_ref, vc_ref, QC, VC))
    ):
        loads[1 + 2 * i].wait()
        loads[2 + 2 * i].wait()
        reduced = jnp.dot(x, basis[...], preferred_element_type=f32).T
        high, low = two_parts(reduced)
        c = cot[...]
        total = jnp.dot(high, c, preferred_element_type=f32) + jnp.dot(
            low, c, preferred_element_type=f32
        )
        for a in range(F):
            for b in range(R):
                at = (a * R + b) * M
                part[b, a, :, start : start + width] = total[at : at + M]

    pl.semaphore_wait(barrier, F + R + T - 3)

    sends = []
    rback = [lax.rem(r + R - k, R) for k in range(R)]
    reach = min(EARLY_FS, F - 1)
    middle_row = rows // 2 // 8 * 8 if SPLIT_EARLY else rows
    tops = [(0, middle_row)] + ([(middle_row, rows)] if middle_row < rows else [])
    near = {}
    for k in range(1, reach + 1):
        for i, (lo, hi) in enumerate(tops if k > 1 else [(0, rows)]):
            near[k, i] = remote(
                w_ref.at[lo:hi], near_ref.at[k - 1, lo:hi], (s8, r8), 2 * k + i, {"fs": zs[k]}
            )
    near_rep = [
        remote(w_ref, near_ref.at[reach + k - 1], (s9, r9), k, {"rep": rs[k]})
        for k in range(1, R)
        if REP_AT
    ]
    sends += list(near.values()) + near_rep
    order = list(range(F - 1, 0, -1)) + [0]
    first = {
        (j, k): remote(
            part.at[rs[k], zs[j]], got1.at[k, j], (s1, r1), (j, k), {"rep": rs[k]}
        )
        for j in order
        for k in range(1, R)
    }
    for c in first.values():
        c.start()
    sends += list(first.values())
    for c in loads[9:]:
        c.wait()
    if REP_AT == 1:
        for c in near_rep:
            c.start()
    for (k, i), c in near.items():
        if i == 0:
            c.start()
    second = {}
    for j in order:
        total = part[r, zs[j]]
        for k in range(1, R):
            first[j, k].wait_recv()
            total = total + got1[k, j]
        if j > 0:
            mid[j] = total
            second[j] = remote(mid.at[j], got2.at[j], (s2, r2), j, {"fs": zs[j]})
            second[j].start()
    sends += list(second.values())
    if REP_AT == 2:
        for c in near_rep:
            c.start()
    for c in loads[5:9]:
        c.wait()
    projected = total
    for j in range(1, F):
        second[j].wait_recv()
        projected = projected + got2[j]

    fn = 0.9 * f_ref[...] + 0.1 * projected
    sn = 0.99 * s_ref[...] + 0.01 * projected * projected
    dirs[z, r] = fn / (jnp.sqrt(sn) + 1e-08)

    third = [remote(dirs.at[z, r], dirs.at[z, r], (s3, r3), k, {"fs": zs[k]}) for k in range(1, F)]
    for c in third:
        c.start()
    for (k, i), c in near.items():
        if i == 1:
            c.start()
    sends += third
    fourth = []
    for j in range(F):
        if j > 0:
            third[j - 1].wait_recv()
        block = dirs.at[back[j], r]
        for k in range(1, R):
            c = remote(block, block, (s4, r4), (j, k), {"rep": rs[k]})
            c.start()
            fourth.append(c)
        if j == 0:
            fn_ref[...] = fn
            sn_ref[...] = sn
    sends += fourth
    for c in fourth:
        c.wait_recv()

    whole = dirs[...].reshape(F * R * M, QC + VC)
    for i, (start, width) in enumerate(((0, QC), (QC, VC))):
        d = whole[:, start : start + width]
        d = (d * d).reshape(F * R * M // 8, 8, width).sum(axis=0)
        acc = d[:, :128]
        for b in range(1, width // 128):
            acc = acc + d[:, b * 128 : (b + 1) * 128]
        squares[i] = acc
    fifth = [remote(squares, squares_in.at[k], (s5, r5), k, {"tp": ts[k]}) for k in range(1, T)]
    for c in fifth:
        c.start()
    sends += fifth

    offset = pl.multiple_of((z * R + r) * rows, rows)
    split_dirs = [three_parts(whole[:, lo : lo + n]) for lo, n in ((0, QC), (QC, VC))]

    def start_of(fs, rep):
        return pl.multiple_of((fs * R + rep) * rows, rows)

    def product(starts):
        results = []
        for basis, (d1, d2, d3) in zip((qb_ref, vb_ref), split_dirs):
            b = jnp.concatenate([basis[pl.ds(at, rows), :] for at in starts], axis=0)
            results.append(
                jnp.dot(b, d1, preferred_element_type=f32)
                + (
                    jnp.dot(b, d2, preferred_element_type=f32)
                    + jnp.dot(b, d3, preferred_element_type=f32)
                )
            )
        return results

    beyond = [start_of(back[k], r) for k in range(1, reach + 1)]
    raw = product([offset] + beyond)
    for c in near.values():
        c.wait_recv()
    for c in fifth:
        c.wait_recv()
    sq = squares[...]
    for k in range(1, T):
        sq = sq + squares_in[k]
    spans = ((0, QC), (QC, VC))
    scales = [
        jnp.sqrt(jnp.sum(sq[i], keepdims=True) / (F * R * M * width * T) + 1.0)
        for i, (start, width) in enumerate(spans)
    ]

    def copy_rows(raw, first, starts, slot):
        for i, (start, width) in enumerate(spans):
            for n, at in enumerate(starts):
                update = raw[i][(first + n) * rows : (first + n + 1) * rows] / scales[i]
                new = near_ref[slot + n, :, start : start + width] - 0.01 * update
                copy_ref[pl.ds(at, rows), start : start + width] = new.astype(bf16)

    for i, (start, width) in enumerate(spans):
        update = raw[i][:rows] / scales[i]
        new = w_ref[:, start : start + width] - 0.01 * update
        copy_ref[pl.ds(offset, rows), start : start + width] = new.astype(bf16)
        u_ref[:, start : start + width] = update
        n_ref[:, start : start + width] = new
    copy_rows(raw, 1, beyond, 0)

    parts = 2 if R == 4 and rows % 32 == 0 else 1
    size = rows // parts

    def piece(j, rep, p):
        at = pl.multiple_of((back[j] * R + rep) * rows + p * size, size)
        return copy_ref.at[pl.ds(at, size), :]

    ready = 1 + reach
    sixth = {}
    for k in range(ready, F):
        for p in range(parts):
            own = piece(0, r, p)
            sixth[k, p] = remote(own, own, (s6, r6), (k, p), {"fs": zs[k]})
            sixth[k, p].start()
    sends += list(sixth.values())

    last = []
    beside = (r + 1 - 2 * lax.rem(r, 2), lax.rem(r + 2, 4))
    direct = {}

    def forward(j):
        for a in range(2):
            direct[j, a, a].wait_recv()
            block = piece(j, beside[a], a)
            c = remote(block, block, (s7, r7), (j, 4 + a), {"rep": beside[1 - a]})
            c.start()
            last.append(c)

    first_block = 1 if REP_AT else 0
    for j in range(first_block, F):
        if REP_AT and j == min(ready, F - 1):
            beside_rows = [start_of(z, rback[k]) for k in range(1, R)]
            raw = product(beside_rows)
            for c in near_rep:
                c.wait_recv()
            copy_rows(raw, 0, beside_rows, reach)
        for p in range(parts):
            if j >= ready:
                sixth[j, p].wait_recv()
            if parts == 1:
                for k in range(1, R):
                    block = piece(j, r, 0)
                    c = remote(block, block, (s7, r7), (j, k), {"rep": rs[k]})
                    c.start()
                    last.append(c)
            elif j >= ready:
                for a in (p, 1 - p):
                    block = piece(j, r, p)
                    direct[j, a, p] = remote(block, block, (s7, r7), (j, a * 2 + p), {"rep": beside[a]})
                    direct[j, a, p].start()
        if parts == 2 and j < ready:
            for a, p in ((0, 0), (1, 1), (0, 1), (1, 0)):
                block = piece(j, r, p)
                direct[j, a, p] = remote(block, block, (s7, r7), (j, a * 2 + p), {"rep": beside[a]})
                direct[j, a, p].start()
        if parts == 2 and j > first_block:
            forward(j - 1)
    if parts == 2:
        forward(F - 1)
    for (j, a, p), c in direct.items():
        if a != p:
            c.wait_recv()
        sends.append(c)
    sends += last
    for c in last:
        c.wait_recv()
    for c in sends:
        c.wait_send()


def write_out(u, n, fn, sn, copy, qu, vu, qn, vn, qfn, qsn, vfn, vsn, qcopy, vcopy, sem):
    QC, VC = qu.shape[1], vu.shape[1]
    query, value = pl.ds(0, QC), pl.ds(QC, VC)
    copies = [
        pltpu.make_async_copy(src.at[:, part], dst, sem.at[i])
        for i, (src, part, dst) in enumerate((
            (copy, value, vcopy),
            (copy, query, qcopy),
            (u, value, vu),
            (n, value, vn),
            (u, query, qu),
            (n, query, qn),
            (fn, query, qfn),
            (fn, value, vfn),
            (sn, query, qsn),
            (sn, value, vsn),
        ))
    ]
    for c in copies:
        c.start()
    for c in copies:
        c.wait()


def fused(plain, *args):
    x, qc, vc, qb, vb, qw, vw, qf, qs, vf, vs = args
    F, R, T = (lax.axis_size(name) for name in ("fs", "rep", "tp"))
    QC, VC = qc.shape[1], vc.shape[1]
    M, rows = qf.shape[0], qw.shape[0]
    aligned = M % 8 == 0 and rows % 16 == 0 and QC % 128 == 0 and VC % 128 == 0
    if not aligned:
        return plain(*args)
    W = QC + VC
    out = jax.ShapeDtypeStruct
    vmem = pl.BlockSpec(memory_space=pltpu.VMEM)
    dma = pltpu.SemaphoreType.DMA
    results = pl.pallas_call(
        functools.partial(kernel, F, R, T),
        out_shape=[
            pltpu.VMEM((rows, W), f32),
            pltpu.VMEM((rows, W), f32),
            pltpu.VMEM((M, W), f32),
            pltpu.VMEM((M, W), f32),
            pltpu.VMEM((rows * F * R, W), bf16),
        ],
        in_specs=[pl.BlockSpec(memory_space=pltpu.HBM)] * 11,
        out_specs=[vmem] * 5,
        scratch_shapes=[
            pltpu.VMEM(x.shape, bf16),
            pltpu.VMEM(qc.shape, bf16),
            pltpu.VMEM(vc.shape, bf16),
            pltpu.VMEM(qb.shape, bf16),
            pltpu.VMEM(vb.shape, bf16),
            pltpu.VMEM((rows, W), f32),
            pltpu.VMEM((M, W), f32),
            pltpu.VMEM((M, W), f32),
            pltpu.VMEM((min(EARLY_FS, F - 1) + R - 1, rows, W), f32),
            pltpu.VMEM((R, F, M, W), f32),
            pltpu.VMEM((R, F, M, W), f32),
            pltpu.VMEM((F, M, W), f32),
            pltpu.VMEM((F, M, W), f32),
            pltpu.VMEM((F, R, M, W), f32),
            pltpu.VMEM((2, 8, 128), f32),
            pltpu.VMEM((T, 2, 8, 128), f32),
            dma((11,)),
            dma((F, R)), dma((F, R)),
            dma((F,)), dma((F,)),
            dma((F,)), dma((F,)),
            dma((F, R)), dma((F, R)),
            dma((T,)), dma((T,)),
            dma((F, 2)), dma((F, 2)),
            dma((F, max(R, 6))), dma((F, max(R, 6))),
            dma((2 * F,)), dma((2 * F,)),
            dma((R,)), dma((R,)),
        ],
        compiler_params=pltpu.CompilerParams(
            collective_id=0, has_side_effects=True, vmem_limit_bytes=VMEM_LIMIT
        ),
    )(*args)
    return tuple(
        pl.pallas_call(
            write_out,
            out_shape=[
                out(qw.shape, f32),
                out(vw.shape, f32),
                out(qw.shape, f32),
                out(vw.shape, f32),
                out(qf.shape, f32),
                out(qf.shape, f32),
                out(vf.shape, f32),
                out(vf.shape, f32),
                out((rows * F * R, QC), bf16),
                out((rows * F * R, VC), bf16),
            ],
            in_specs=[vmem] * 5,
            out_specs=[pl.BlockSpec(memory_space=pltpu.HBM)] * 10,
            scratch_shapes=[dma((10,))],
            compiler_params=pltpu.CompilerParams(vmem_limit_bytes=OUT_LIMIT),
        )(*results)
    )


def solution(mesh):
    in_specs = (
        P(("fs", "rep"), None),
        P(("fs", "rep"), "tp"),
        P(("fs", "rep"), "tp"),
        P(),
        P(),
        P(("fs", "rep"), "tp"),
        P(("fs", "rep"), "tp"),
        P(("fs", "rep"), "tp"),
        P(("fs", "rep"), "tp"),
        P(("fs", "rep"), "tp"),
        P(("fs", "rep"), "tp"),
    )
    out_specs = (
        P(("fs", "rep"), "tp"),
        P(("fs", "rep"), "tp"),
        P(("fs", "rep"), "tp"),
        P(("fs", "rep"), "tp"),
        P(("fs", "rep"), "tp"),
        P(("fs", "rep"), "tp"),
        P(("fs", "rep"), "tp"),
        P(("fs", "rep"), "tp"),
        P(None, "tp"),
        P(None, "tp"),
    )
    return jax.shard_map(functools.partial(fused, body), mesh=mesh, in_specs=in_specs, out_specs=out_specs, check_vma=False)
```

profile of v0, /device:TPU:0, one launch (start us, length us, event | category | flops | bytes accessed | tf_op | source)
XLA Modules:
  0.0 42.2 jit_solution(2147925654153087010)
XLA Ops:
  0.6 40.2 %shard_map.186 = (f32[64,768]{1,0:T(8,128)S(1)}, f32[64,768]{1,0:T(8,128)S(1)}, f32[8,768]{1,0:T(8,128)S(1)}, f32[8,768]{1,0:T(8,128)S(1)}, bf16[1024,768]{1,0:T(8,128)(2,1)S(1)}) custom-call(bf16[128,1024]{1,0:T(8,128)(2,1)} %x_hbm.1, bf16[128,256]{1,0:T(8,128)(2,1)} %qc_hbm.1, bf16[128,512]{1,0:T(8,128)(2,1)} %vc_hbm.1, bf16[1024,128]{1,0:T(8,128)(2,1)} %qb_hbm.1, ...), custom_call_target="tpu_custom_call" | custom-call | tf_op jit(solution)/shard_map/pallas_call | solution.py:469
  40.9 1.4 %shard_map.187 = (f32[64,256]{1,0:T(8,128)}, f32[64,512]{1,0:T(8,128)}, f32[64,256]{1,0:T(8,128)}, f32[64,512]{1,0:T(8,128)}, f32[8,256]{1,0:T(8,128)}, /*index=...) custom-call(f32[64,768]{1,0:T(8,128)S(1)} %get-tuple-element.15.u, ...), custom_call_target="tpu_custom_call" | custom-call | tf_op jit(solution)/shard_map/pallas_call | solution.py:513
where the time goes:
time: 42.4 us; the launch traced here: 42.2 us
  Pallas kernels  41.6 us (98%)
  between operations  0.65 us (2%)
    pallas_call x1, Pallas kernels, fused(): pl.pallas_call(functools.partial(kernel, F, R, T), out_shape=[pltpu.VMEM(...  40.2 us
    pallas_call x1, Pallas kernels, fused(): pl.pallas_call(write_out, out_shape=[out(qw.shape, f32), out(vw.shape, f3...  1.36 us

commit v1 on v0

v1 whole, which is shorter than its diff:
```python
import functools
import jax
import jax.numpy as jnp
from jax import lax
from jax.experimental import pallas as pl
from jax.experimental.pallas import tpu as pltpu
from jax.sharding import PartitionSpec as P


def moments(projected, first_old, second_old):
    first_new = 0.9 * first_old + 0.1 * projected
    second_new = 0.99 * second_old + 0.01 * projected * projected
    return (first_new, second_new, first_new / (jnp.sqrt(second_new) + 1e-08))


def finish(whole_dir, basis_rows, weight, squares, entries):
    norm_scale = jnp.sqrt(squares / entries + 1.0)
    update = jnp.dot(basis_rows, whole_dir, precision=lax.Precision.HIGHEST) / norm_scale
    weight_new = weight - 0.01 * update
    return (update, weight_new, weight_new.astype(jnp.bfloat16))


def split_parts(reduced):
    high_part = reduced.astype(jnp.bfloat16)
    held = lax.optimization_barrier(high_part)
    low_part = (reduced - held.astype(jnp.float32)).astype(jnp.bfloat16)
    return (high_part, low_part)


def parts_product(high_part, low_part, cotangent):
    dims = (((0,), (0,)), ((), ()))
    first_term = lax.dot_general(high_part, cotangent, dims, preferred_element_type=jnp.float32)
    second_term = lax.dot_general(low_part, cotangent, dims, preferred_element_type=jnp.float32)
    return first_term + second_term


def body(
    normed_input,
    query_cotangent,
    value_cotangent,
    query_basis,
    value_basis,
    query_weight,
    value_weight,
    query_first,
    query_second,
    value_first,
    value_second,
):
    row_count = query_weight.shape[0]
    query_width = query_cotangent.shape[1]
    offset = lax.axis_index(("fs", "rep")) * row_count
    query_rows = lax.dynamic_slice_in_dim(query_basis, offset, row_count, 0).astype(jnp.float32)
    value_rows = lax.dynamic_slice_in_dim(value_basis, offset, row_count, 0).astype(jnp.float32)
    reduced_query = jnp.dot(normed_input, query_basis, preferred_element_type=jnp.float32)
    reduced_value = jnp.dot(normed_input, value_basis, preferred_element_type=jnp.float32)
    query_high, query_low = split_parts(reduced_query)
    value_high, value_low = split_parts(reduced_value)
    projected = lax.psum_scatter(
        jnp.concatenate(
            [
                parts_product(query_high, query_low, query_cotangent),
                parts_product(value_high, value_low, value_cotangent),
            ],
            axis=1,
        ),
        ("fs", "rep"),
        scatter_dimension=0,
        tiled=True,
    )
    query_projected = projected[:, :query_width]
    value_projected = projected[:, query_width:]
    query_first_new, query_second_new, query_dir = moments(
        query_projected, query_first, query_second
    )
    value_first_new, value_second_new, value_dir = moments(
        value_projected, value_first, value_second
    )
    query_whole, value_whole = (
        lax.all_gather(query_dir, ("fs", "rep"), axis=0, tiled=True),
        lax.all_gather(value_dir, ("fs", "rep"), axis=0, tiled=True),
    )
    query_squares, value_squares = lax.psum(
        (jnp.sum(query_dir * query_dir), jnp.sum(value_dir * value_dir)), ("fs", "rep", "tp")
    )
    tp_count = lax.axis_size("tp")
    query_update, query_weight_new, query_half = finish(
        query_whole,
        query_rows,
        query_weight,
        query_squares,
        query_whole.shape[0] * query_whole.shape[1] * tp_count,
    )
    value_update, value_weight_new, value_half = finish(
        value_whole,
        value_rows,
        value_weight,
        value_squares,
        value_whole.shape[0] * value_whole.shape[1] * tp_count,
    )
    query_copy, value_copy = (
        lax.all_gather(query_half, ("fs", "rep"), axis=0, tiled=True),
        lax.all_gather(value_half, ("fs", "rep"), axis=0, tiled=True),
    )
    return (
        query_update,
        value_update,
        query_weight_new,
        value_weight_new,
        query_first_new,
        query_second_new,
        value_first_new,
        value_second_new,
        query_copy,
        value_copy,
    )


MESH = pl.DeviceIdType.MESH
VMEM_LIMIT = 60 * 2**20
OUT_LIMIT = 16 * 2**20
CHUNKS = (0, 1)
EARLY_Z = (1, 2)
OFF_Z = True
PLAN = {
    "sent": (("z", 1, 0), ("z", 1, 1)),
    "second0": (("r", 0, 0), ("r", 1, 0)),
    "second1": (("r", 0, 1), ("r", 1, 1)),
    "third0": (("z", 2, 0),),
    "third1": (("z", 2, 1),),
}
f32, bf16 = jnp.float32, jnp.bfloat16


def scope(name):
    pass


def two_parts(x):
    high = x.astype(bf16)
    return high, (x - high.astype(f32)).astype(bf16)


def size_of(ref):
    n = jnp.dtype(ref.dtype).itemsize
    for d in ref.shape:
        n *= d
    return n


def kernel(
    T,
    x_hbm, qc_hbm, vc_hbm, qb_hbm, vb_hbm, qw_hbm, vw_hbm, qf_hbm, qs_hbm, vf_hbm, vs_hbm,
    qu, vu, qn, vn, qfn, vfn, qsn, vsn, qcopy, vcopy,
    x_ref, qc, vc, qb, vb, qw, vw, qf, vf, qs, vs,
    qzw, vzw, qrw, vrw, qpart, vpart, qgot1, vgot1, qmid, vmid, qgot2, vgot2, qdirs, vdirs,
    qsq, vsq, qsq_in, vsq_in, spare,
    load, sent, in1, in2, in3, in4, in5, in6, in7, in8, in9, in10, rest,
):
    F, R = 4, 4
    z, r, t = lax.axis_index("fs"), lax.axis_index("rep"), lax.axis_index("tp")
    zs = [z, z + 1 - 2 * lax.rem(z, 2), 3 - z, lax.rem(z + 2, 4)]
    rs = [r, r + 1 - 2 * lax.rem(r, 2), lax.rem(r + 2, 4), 3 - r]
    ts = [lax.rem(t + k, T) for k in range(T)]
    rows, M = qw.shape[0], qf.shape[0]
    cot, basis, weight, first, second = (qc, vc), (qb, vb), (qw, vw), (qf, vf), (qs, vs)
    update_out, weight_out, first_out, second_out = (qu, vu), (qn, vn), (qfn, vfn), (qsn, vsn)
    copy, z_weight, r_weight = (qcopy, vcopy), (qzw, vzw), (qrw, vrw)
    part, got1, mid, got2, dirs = (qpart, vpart), (qgot1, vgot1), (qmid, vmid), (qgot2, vgot2), (qdirs, vdirs)
    squares, squares_in = (qsq, vsq), (qsq_in, vsq_in)
    width = [w.shape[1] for w in weight]

    total_sent, total_rest = [], []

    def remote(src, dst, received, peer, last=False):
        d = pltpu.make_async_remote_copy(
            src_ref=src,
            dst_ref=dst,
            send_sem=sent.at[0],
            recv_sem=received,
            device_id=peer,
            device_id_type=MESH,
        )
        d.start()
        total_sent.append(size_of(src))
        if last:
            total_rest.append(size_of(src))
        return d

    def settle(ref, sem):
        pltpu.make_async_copy(ref, ref, sem).wait()

    scope("p00_sig_load")
    barrier = pltpu.get_barrier_semaphore()
    for axis, others in (("rep", rs), ("fs", zs), ("tp", ts)):
        for other in others[1:]:
            pl.semaphore_signal(barrier, inc=1, device_id={axis: other}, device_id_type=MESH)
    sources = {
        "x": (x_hbm, x_ref),
        ("basis", 0): (qb_hbm, qb), ("cot", 0): (qc_hbm, qc),
        ("basis", 1): (vb_hbm, vb), ("cot", 1): (vc_hbm, vc),
        ("weight", 0): (qw_hbm, qw), ("weight", 1): (vw_hbm, vw),
        ("first", 0): (qf_hbm, qf), ("first", 1): (vf_hbm, vf),
        ("second", 0): (qs_hbm, qs), ("second", 1): (vs_hbm, vs),
    }
    names = ["x"] + [(n, c) for c in CHUNKS for n in ("basis", "cot")]
    names += [(n, c) for n in ("weight", "first", "second") for c in CHUNKS]
    loads = {
        n: pltpu.make_async_copy(sources[n][0], sources[n][1], load.at[i])
        for i, n in enumerate(names)
    }
    for c in loads.values():
        c.start()

    early = {}

    def run(point):
        for kind, k, c in PLAN.get(point, ()):
            if ("weight", c) in loads:
                loads.pop(("weight", c)).wait()
            if kind == "z":
                d = remote(weight[c], z_weight[c].at[k - 1], in8.at[c, k - 1], {"fs": zs[k]})
            else:
                d = remote(weight[c], r_weight[c].at[k], in9.at[c, k], {"rep": rs[k + 1]})
            early[kind, k, c] = d

    far = (2, 3, 1, 0)
    for i, c in enumerate(CHUNKS):
        scope(f"p01_load_dot#c={c}")
        if i == 0:
            loads.pop("x").wait()
            x = x_ref[...]
        loads.pop(("basis", c)).wait()
        reduced = jnp.dot(x, basis[c][...], preferred_element_type=f32).T
        high, low = two_parts(reduced)
        both = jnp.concatenate([high, low], axis=1)
        loads.pop(("cot", c)).wait()
        g = cot[c][...]
        total = jnp.dot(both, jnp.concatenate([g, g], axis=0), preferred_element_type=f32)
        for a in range(F):
            for b in range(R):
                at = (a * R + b) * M
                part[c][b, a] = total[at : at + M]
        if i == 0:
            scope("p02_barrier")
            pl.semaphore_wait(barrier, F + R + T - 3)
        scope(f"p03_send1#c={c}")
        for j in far:
            for k in range(1, R):
                remote(part[c].at[rs[k], zs[j]], got1[c].at[k, j], in1.at[c, j], {"rep": rs[k]})
    run("sent")

    own = {}
    for c in CHUNKS:
        scope(f"p04_recv1#c={c}")
        for j in far:
            total = part[c][r, zs[j]]
            settle(got1[c].at[1:R, j], in1.at[c, j])
            for k in range(1, R):
                total = total + got1[c][k, j]
            if j > 0:
                mid[c][j] = total
                remote(mid[c].at[j], got2[c].at[j], in2.at[c], {"fs": zs[j]})
            else:
                own[c] = total
        run(f"second{c}")

    third = {}

    def spread(c, j):
        block = dirs[c].at[zs[j], r]
        for k in range(1, R):
            remote(block, block, in4.at[c], {"rep": rs[k]})

    for c in CHUNKS:
        scope(f"p05_recv2#c={c}")
        loads.pop(("first", c)).wait()
        loads.pop(("second", c)).wait()
        projected = own[c]
        settle(got2[c].at[1:F], in2.at[c])
        for j in (1, 3, 2):
            projected = projected + got2[c][j]
        fn = 0.9 * first[c][...] + 0.1 * projected
        sn = 0.99 * second[c][...] + 0.01 * projected * projected
        dirs[c][z, r] = fn / (jnp.sqrt(sn) + 1e-08)
        block = dirs[c].at[z, r]
        for j in (2, 3, 1):
            third[c, j] = remote(block, block, in3.at[c, j - 1], {"fs": zs[j]})
        spread(c, 0)
        first_out[c][...] = fn
        second_out[c][...] = sn
        run(f"third{c}")

    for c in CHUNKS:
        scope(f"p06_recv3#c={c}")
        for j in (1, 3, 2):
            third[c, j].wait_recv()
            spread(c, j)
        run(f"fourth{c}")

    def start_of(j, k):
        return pl.multiple_of((zs[j] * R + rs[k]) * rows, rows)

    size = rows // 2

    def piece(c, j, k, p):
        at = pl.multiple_of(start_of(j, k) + p * size, size)
        return copy[c].at[pl.ds(at, size), :]

    def product(c, dd, blocks):
        b = jnp.concatenate([basis[c][pl.ds(start_of(j, k), rows), :] for j, k in blocks], axis=0)
        return jnp.dot(jnp.concatenate([b, b], axis=1), dd, preferred_element_type=f32)

    direct, across, sixth = {}, {}, {}

    def pass_on(c, j, a):
        block = piece(c, j, a + 1, a)
        remote(block, block, rest.at[0], {"rep": rs[2 - a]}, True)

    def send_direct(c, j, order=((0, 0), (1, 1), (0, 1), (1, 0))):
        for a, p in order:
            block = piece(c, j, 0, p)
            if a == p:
                direct[c, j, a] = remote(block, block, in7.at[c, j - 1, a], {"rep": rs[a + 1]})
            else:
                remote(block, block, rest.at[0], {"rep": rs[a + 1]}, True)

    late = [j for j in range(1, F) if j not in EARLY_Z]
    for c in CHUNKS:
        scope(f"p07_recv4#c={c}")
        settle(dirs[c].at[:, 1:R], in4.at[c])
        scope(f"p08_square#c={c}")
        whole = dirs[c][...].reshape(F * R * M, width[c])
        d = (whole * whole).reshape(F * R * M // 8, 8, width[c]).sum(axis=0)
        acc = d[:, :128]
        for b in range(1, width[c] // 128):
            acc = acc + d[:, b * 128 : (b + 1) * 128]
        squares[c][...] = acc
        for k in range(1, T):
            remote(squares[c], squares_in[c].at[k], in5.at[c], {"tp": ts[k]})
        dd = jnp.concatenate(two_parts(whole), axis=0)
        lines = [(0, 0)] + [(k, 0) for k in EARLY_Z]
        raw = product(c, dd, lines)
        sides = [(0, 1), (0, 2)]
        raw_side = product(c, dd, sides)
        scope(f"p09_fifth#c={c}")
        settle(squares_in[c].at[1:T], in5.at[c])
        sq = squares[c][...]
        for k in range(1, T):
            sq = sq + squares_in[c][k]
        scale = jnp.sqrt(jnp.sum(sq, keepdims=True) / (F * R * M * width[c] * T) + 1.0)
        inverse = 1.0 / scale
        if ("weight", c) in loads:
            loads.pop(("weight", c)).wait()
        scope(f"p10_copy#c={c}")
        for n, (j, k) in enumerate(lines):
            update = raw[n * rows : (n + 1) * rows] * inverse
            if n == 0:
                new = weight[c][...] - 0.01 * update
                update_out[c][...] = update
                weight_out[c][...] = new
            else:
                early["z", j, c].wait_recv()
                new = z_weight[c][j - 1] - 0.01 * update
            copy[c][pl.ds(start_of(j, k), rows), :] = new.astype(bf16)
            if n == 0:
                for j2 in late:
                    block = copy[c].at[pl.ds(start_of(0, 0), rows), :]
                    sixth[c, j2] = remote(block, block, in6.at[c, j2 - 1], {"fs": zs[j2]})
            elif not (OFF_Z and j == 1):
                send_direct(c, j)
        scope(f"p11_side#c={c}")
        for n, (j, k) in enumerate(sides):
            update = raw_side[n * rows : (n + 1) * rows] * inverse
            early["r", n, c].wait_recv()
            new = r_weight[c][n] - 0.01 * update
            copy[c][pl.ds(start_of(j, k), rows), :] = new.astype(bf16)
            if OFF_Z:
                block = piece(c, 0, k, n)
                across[c, n] = remote(block, block, in10.at[c, n], {"fs": zs[1]})
                block = piece(c, 0, k, 1 - n)
                remote(block, block, rest.at[0], {"fs": zs[1]}, True)
        for a in range(2):
            pass_on(c, 0, a)
        run(f"final{c}")

    for c in CHUNKS:
        scope(f"p12_sixth#c={c}")
        for j in late:
            sixth[c, j].wait_recv()
            send_direct(c, j)
    for c in CHUNKS:
        for j in range(1, F):
            if j in late:
                continue
            scope(f"p13_pass#c={c}#j={j}")
            for a in range(2):
                (across[c, a] if OFF_Z and j == 1 else direct[c, j, a]).wait_recv()
                pass_on(c, j, a)
    for c in CHUNKS:
        for j in late:
            scope(f"p14_pass#c={c}#j={j}")
            for a in range(2):
                direct[c, j, a].wait_recv()
                pass_on(c, j, a)
    scope("p15_last")
    settle(spare.at[: sum(total_rest) // 512], rest.at[0])
    scope("p16_waitsend")
    settle(spare.at[: sum(total_sent) // 512], sent.at[0])
    scope(None)


def write_out(*refs):
    sem, sources, targets = refs[20], refs[:10], refs[10:20]
    copies = [
        pltpu.make_async_copy(src, dst, sem.at[i])
        for i, (src, dst) in enumerate(zip(sources, targets))
    ]
    for c in copies[::-1]:
        c.start()
    for c in copies[::-1]:
        c.wait()


def fused(plain, *args):
    x, qc, vc, qb, vb, qw, vw, qf, qs, vf, vs = args
    F, R, T = (lax.axis_size(name) for name in ("fs", "rep", "tp"))
    QC, VC = qc.shape[1], vc.shape[1]
    M, rows = qf.shape[0], qw.shape[0]
    aligned = M % 8 == 0 and rows % 32 == 0 and QC % 128 == 0 and VC % 128 == 0
    if not aligned or F != 4 or R != 4:
        return plain(*args)
    out = jax.ShapeDtypeStruct
    vmem = pl.BlockSpec(memory_space=pltpu.VMEM)
    dma = pltpu.SemaphoreType.DMA
    W = (QC, VC)

    def each(*shape, dtype=f32):
        return [pltpu.VMEM(shape + (w,), dtype) for w in W]

    sems = [
        (11,), (1,), (2, F), (2,), (2, F - 1), (2,), (2,), (2, F - 1), (2, F - 1, 2), (2, F - 1), (2, 2), (2, 2), (1,),
    ]
    results = pl.pallas_call(
        functools.partial(kernel, T),
        out_shape=each(rows) + each(rows) + each(M) + each(M) + each(rows * F * R, dtype=bf16),
        in_specs=[pl.BlockSpec(memory_space=pltpu.HBM)] * 11,
        out_specs=[vmem] * 10,
        scratch_shapes=[
            pltpu.VMEM(x.shape, bf16),
            pltpu.VMEM(qc.shape, bf16),
            pltpu.VMEM(vc.shape, bf16),
            pltpu.VMEM(qb.shape, bf16),
            pltpu.VMEM(vb.shape, bf16),
            *each(rows), *each(M), *each(M),
            *each(F - 1, rows), *each(2, rows),
            *each(R, F, M), *each(R, F, M), *each(F, M), *each(F, M), *each(F, R, M),
            pltpu.VMEM((8, 128), f32), pltpu.VMEM((8, 128), f32),
            pltpu.VMEM((T, 8, 128), f32), pltpu.VMEM((T, 8, 128), f32),
            pltpu.VMEM((8 * rows * F * R, 128), f32),
            *[dma(shape) for shape in sems],
        ],
        compiler_params=pltpu.CompilerParams(
            collective_id=0, has_side_effects=True, vmem_limit_bytes=VMEM_LIMIT
        ),
    )(*args)
    outs = pl.pallas_call(
        write_out,
        out_shape=[
            out(qw.shape, f32), out(vw.shape, f32), out(qw.shape, f32), out(vw.shape, f32),
            out(qf.shape, f32), out(vf.shape, f32), out(qf.shape, f32), out(vf.shape, f32),
            out((rows * F * R, QC), bf16), out((rows * F * R, VC), bf16),
        ],
        in_specs=[vmem] * 10,
        out_specs=[pl.BlockSpec(memory_space=pltpu.HBM)] * 10,
        scratch_shapes=[dma((10,))],
        compiler_params=pltpu.CompilerParams(vmem_limit_bytes=OUT_LIMIT),
    )(*results)
    qu, vu, qn, vn, qfn, vfn, qsn, vsn, qcopy, vcopy = outs
    return (qu, vu, qn, vn, qfn, qsn, vfn, vsn, qcopy, vcopy)


def solution(mesh):
    in_specs = (
        P(("fs", "rep"), None),
        P(("fs", "rep"), "tp"),
        P(("fs", "rep"), "tp"),
        P(),
        P(),
        P(("fs", "rep"), "tp"),
        P(("fs", "rep"), "tp"),
        P(("fs", "rep"), "tp"),
        P(("fs", "rep"), "tp"),
        P(("fs", "rep"), "tp"),
        P(("fs", "rep"), "tp"),
    )
    out_specs = (
        P(("fs", "rep"), "tp"),
        P(("fs", "rep"), "tp"),
        P(("fs", "rep"), "tp"),
        P(("fs", "rep"), "tp"),
        P(("fs", "rep"), "tp"),
        P(("fs", "rep"), "tp"),
        P(("fs", "rep"), "tp"),
        P(("fs", "rep"), "tp"),
        P(None, "tp"),
        P(None, "tp"),
    )
    return jax.shard_map(functools.partial(fused, body), mesh=mesh, in_specs=in_specs, out_specs=out_specs, check_vma=False)
```

time: 42.4 us -> 39.5 us (0.932)
  Pallas kernels: 41.6 us -> 38.7 us
    pallas_call x1, Pallas kernels: 40.2 us -> 37.3 us  [fused(): pl.pallas_call(functools.partial(kernel, T), out_shape=each(rows) + each(...]
where the time goes in v1:
time: 39.5 us; the launch traced here: 39.4 us
  Pallas kernels  38.7 us (98%)
  between operations  0.65 us (2%)
    pallas_call x1, Pallas kernels, fused(): pl.pallas_call(functools.partial(kernel, T), out_shape=each(rows) + each(...  37.3 us
    pallas_call x1, Pallas kernels, fused(): pl.pallas_call(write_out, out_shape=[out(qw.shape, f32), out(vw.shape, f3...  1.37 us

profile of v1, /device:TPU:0, one launch (start us, length us, event | category | flops | bytes accessed | tf_op | source)
XLA Modules:
  0.0 39.4 jit_solution(13185638672514324395)
XLA Ops:
  0.6 37.3 %shard_map.186 = (f32[64,256]{1,0:T(8,128)S(1)}, f32[64,512]{1,0:T(8,128)S(1)}, f32[64,256]{1,0:T(8,128)S(1)}, f32[64,512]{1,0:T(8,128)S(1)}, f32[8,256]{1,0:T(8...) custom-call(bf16[128,1024]{1,0:T(8,128)(2,1)} %x_hbm.1, ...), custom_call_target="tpu_custom_call" | custom-call | tf_op jit(solution)/shard_map/pallas_call | solution.py:444
  38.0 1.4 %shard_map.187 = (f32[64,256]{1,0:T(8,128)}, f32[64,512]{1,0:T(8,128)}, f32[64,256]{1,0:T(8,128)}, f32[64,512]{1,0:T(8,128)}, f32[8,256]{1,0:T(8,128)}, /*index=...) custom-call(f32[64,256]{1,0:T(8,128)S(1)} %get-tuple-element.30.refs, ...), custom_call_target="tpu_custom_call" | custom-call | tf_op jit(solution)/shard_map/pallas_call | solution.py:467

commit v2 on v1

--- a/solution.py
+++ b/solution.py
@@ -122,13 +122,7 @@
 CHUNKS = (0, 1)
 EARLY_Z = (1, 2)
 OFF_Z = True
-PLAN = {
-    "sent": (("z", 1, 0), ("z", 1, 1)),
-    "second0": (("r", 0, 0), ("r", 1, 0)),
-    "second1": (("r", 0, 1), ("r", 1, 1)),
-    "third0": (("z", 2, 0),),
-    "third1": (("z", 2, 1),),
-}
+PLAN = {'sent': (('z', 2, 0), ('z', 1, 1)), 'second0': (('r', 0, 0), ('r', 1, 0)), 'second1': (('r', 0, 1), ('r', 1, 1)), 'fourth1': (('z', 1, 0), ('z', 2, 1))}
 f32, bf16 = jnp.float32, jnp.bfloat16
 
 
@@ -154,7 +148,7 @@
     qu, vu, qn, vn, qfn, vfn, qsn, vsn, qcopy, vcopy,
     x_ref, qc, vc, qb, vb, qw, vw, qf, vf, qs, vs,
     qzw, vzw, qrw, vrw, qpart, vpart, qgot1, vgot1, qmid, vmid, qgot2, vgot2, qdirs, vdirs,
-    qsq, vsq, qsq_in, vsq_in, spare,
+    norms, spare,
     load, sent, in1, in2, in3, in4, in5, in6, in7, in8, in9, in10, rest,
 ):
     F, R = 4, 4
@@ -167,7 +161,6 @@
     update_out, weight_out, first_out, second_out = (qu, vu), (qn, vn), (qfn, vfn), (qsn, vsn)
     copy, z_weight, r_weight = (qcopy, vcopy), (qzw, vzw), (qrw, vrw)
     part, got1, mid, got2, dirs = (qpart, vpart), (qgot1, vgot1), (qmid, vmid), (qgot2, vgot2), (qdirs, vdirs)
-    squares, squares_in = (qsq, vsq), (qsq_in, vsq_in)
     width = [w.shape[1] for w in weight]
 
     total_sent, total_rest = [], []
@@ -265,7 +258,7 @@
                 own[c] = total
         run(f"second{c}")
 
-    third = {}
+    third, sums = {}, []
 
     def spread(c, j):
         block = dirs[c].at[zs[j], r]
@@ -283,6 +276,19 @@
         fn = 0.9 * first[c][...] + 0.1 * projected
         sn = 0.99 * second[c][...] + 0.01 * projected * projected
         dirs[c][z, r] = fn / (jnp.sqrt(sn) + 1e-08)
+        sums.append(jnp.sum(dirs[c][z, r] * dirs[c][z, r], keepdims=True))
+        if c == CHUNKS[-1]:
+            scope("p055_norms")
+            lane = lax.broadcasted_iota(jnp.int32, (1, 128), 1)
+            slot = (z * R + r) * T + t
+            norms[slot] = jnp.where(lane < 64, sums[CHUNKS.index(0)], sums[CHUNKS.index(1)])
+            for j in far:
+                for k in range(R):
+                    for n in range(T):
+                        if j or k or n:
+                            peer = {"fs": zs[j], "rep": rs[k], "tp": ts[n]}
+                            remote(norms.at[slot], norms.at[slot], in5.at[0], peer)
+            scope(f"p056_third#c={c}")
         block = dirs[c].at[z, r]
         for j in (2, 3, 1):
             third[c, j] = remote(block, block, in3.at[c, j - 1], {"fs": zs[j]})
@@ -326,63 +332,62 @@
                 remote(block, block, rest.at[0], {"rep": rs[a + 1]}, True)
 
     late = [j for j in range(1, F) if j not in EARLY_Z]
+    waiting = []
     for c in CHUNKS:
         scope(f"p07_recv4#c={c}")
         settle(dirs[c].at[:, 1:R], in4.at[c])
         scope(f"p08_square#c={c}")
         whole = dirs[c][...].reshape(F * R * M, width[c])
-        d = (whole * whole).reshape(F * R * M // 8, 8, width[c]).sum(axis=0)
-        acc = d[:, :128]
-        for b in range(1, width[c] // 128):
-            acc = acc + d[:, b * 128 : (b + 1) * 128]
-        squares[c][...] = acc
-        for k in range(1, T):
-            remote(squares[c], squares_in[c].at[k], in5.at[c], {"tp": ts[k]})
         dd = jnp.concatenate(two_parts(whole), axis=0)
-        lines = [(0, 0)] + [(k, 0) for k in EARLY_Z]
-        raw = product(c, dd, lines)
-        sides = [(0, 1), (0, 2)]
-        raw_side = product(c, dd, sides)
+        blocks = [(0, 0), (1, 0), (0, 1), (0, 2)] + [(j, 0) for j in EARLY_Z if j > 1]
+        raw = product(c, dd, blocks[:4])
+        raw_far = product(c, dd, blocks[4:]) if blocks[4:] else None
         scope(f"p09_fifth#c={c}")
-        settle(squares_in[c].at[1:T], in5.at[c])
-        sq = squares[c][...]
-        for k in range(1, T):
-            sq = sq + squares_in[c][k]
-        scale = jnp.sqrt(jnp.sum(sq, keepdims=True) / (F * R * M * width[c] * T) + 1.0)
-        inverse = 1.0 / scale
+        if c == CHUNKS[0]:
+            settle(spare.at[: F * R * T - 1], in5.at[0])
+            sq = jnp.sum(norms[...].reshape(F * R * T, 128), axis=0, keepdims=True)
+        count = F * R * M * width[c] * T
+        inverse = 1.0 / jnp.sqrt(sq[:, 64 * c : 64 * c + 1] / count + 1.0)
         if ("weight", c) in loads:
             loads.pop(("weight", c)).wait()
         scope(f"p10_copy#c={c}")
-        for n, (j, k) in enumerate(lines):
-            update = raw[n * rows : (n + 1) * rows] * inverse
+        for n, (j, k) in enumerate(blocks):
+            source = raw if n < 4 else raw_far
+            update = source[n % 4 * rows : (n % 4 + 1) * rows] * inverse
             if n == 0:
                 new = weight[c][...] - 0.01 * update
                 update_out[c][...] = update
                 weight_out[c][...] = new
-            else:
+            elif k == 0:
+                if j > 1:
+                    waiting.append((c, j, update))
+                    continue
                 early["z", j, c].wait_recv()
                 new = z_weight[c][j - 1] - 0.01 * update
+            else:
+                early["r", k - 1, c].wait_recv()
+                new = r_weight[c][k - 1] - 0.01 * update
             copy[c][pl.ds(start_of(j, k), rows), :] = new.astype(bf16)
             if n == 0:
                 for j2 in late:
                     block = copy[c].at[pl.ds(start_of(0, 0), rows), :]
                     sixth[c, j2] = remote(block, block, in6.at[c, j2 - 1], {"fs": zs[j2]})
-            elif not (OFF_Z and j == 1):
+            elif k == 0 and not OFF_Z:
                 send_direct(c, j)
-        scope(f"p11_side#c={c}")
-        for n, (j, k) in enumerate(sides):
-            update = raw_side[n * rows : (n + 1) * rows] * inverse
-            early["r", n, c].wait_recv()
-            new = r_weight[c][n] - 0.01 * update
-            copy[c][pl.ds(start_of(j, k), rows), :] = new.astype(bf16)
-            if OFF_Z:
-                block = piece(c, 0, k, n)
-                across[c, n] = remote(block, block, in10.at[c, n], {"fs": zs[1]})
-                block = piece(c, 0, k, 1 - n)
+            elif k > 0 and OFF_Z:
+                block = piece(c, 0, k, k - 1)
+                across[c, k - 1] = remote(block, block, in10.at[c, k - 1], {"fs": zs[1]})
+                block = piece(c, 0, k, 2 - k)
                 remote(block, block, rest.at[0], {"fs": zs[1]}, True)
         for a in range(2):
             pass_on(c, 0, a)
         run(f"final{c}")
+    for c, j, update in waiting:
+        scope(f"p115_far#c={c}")
+        early["z", j, c].wait_recv()
+        new = z_weight[c][j - 1] - 0.01 * update
+        copy[c][pl.ds(start_of(j, 0), rows), :] = new.astype(bf16)
+        send_direct(c, j)
 
     for c in CHUNKS:
         scope(f"p12_sixth#c={c}")
@@ -439,7 +444,7 @@
         return [pltpu.VMEM(shape + (w,), dtype) for w in W]
 
     sems = [
-        (11,), (1,), (2, F), (2,), (2, F - 1), (2,), (2,), (2, F - 1), (2, F - 1, 2), (2, F - 1), (2, 2), (2, 2), (1,),
+        (11,), (1,), (2, F), (2,), (2, F - 1), (2,), (1,), (2, F - 1), (2, F - 1, 2), (2, F - 1), (2, 2), (2, 2), (1,),
     ]
     results = pl.pallas_call(
         functools.partial(kernel, T),
@@ -455,8 +460,7 @@
             *each(rows), *each(M), *each(M),
             *each(F - 1, rows), *each(2, rows),
             *each(R, F, M), *each(R, F, M), *each(F, M), *each(F, M), *each(F, R, M),
-            pltpu.VMEM((8, 128), f32), pltpu.VMEM((8, 128), f32),
-            pltpu.VMEM((T, 8, 128), f32), pltpu.VMEM((T, 8, 128), f32),
+            pltpu.VMEM((F * R * T, 1, 128), f32),
             pltpu.VMEM((8 * rows * F * R, 128), f32),
             *[dma(shape) for shape in sems],
         ],

time: 39.5 us -> 37.2 us (0.942)
  Pallas kernels: 38.7 us -> 36.4 us
    pallas_call x1, Pallas kernels: 37.3 us -> 35 us  [fused(): pl.pallas_call(functools.partial(kernel, T), out_shape=each(rows) + each(...]
where the time goes in v2:
time: 37.2 us; the launch traced here: 37 us
  Pallas kernels  36.4 us (98%)
  between operations  0.65 us (2%)
    pallas_call x1, Pallas kernels, fused(): pl.pallas_call(functools.partial(kernel, T), out_shape=each(rows) + each(...  35 us
    pallas_call x1, Pallas kernels, fused(): pl.pallas_call(write_out, out_shape=[out(qw.shape, f32), out(vw.shape, f3...  1.37 us

profile of v2, /device:TPU:0, one launch (start us, length us, event | category | flops | bytes accessed | tf_op | source)
XLA Modules:
  0.0 37.0 jit_solution(3550706103313203263)
XLA Ops:
  0.6 35.0 %shard_map.186 = (f32[64,256]{1,0:T(8,128)S(1)}, f32[64,512]{1,0:T(8,128)S(1)}, f32[64,256]{1,0:T(8,128)S(1)}, f32[64,512]{1,0:T(8,128)S(1)}, f32[8,256]{1,0:T(8...) custom-call(bf16[128,1024]{1,0:T(8,128)(2,1)} %x_hbm.1, ...), custom_call_target="tpu_custom_call" | custom-call | tf_op jit(solution)/shard_map/pallas_call | solution.py:449
  35.7 1.4 %shard_map.187 = (f32[64,256]{1,0:T(8,128)}, f32[64,512]{1,0:T(8,128)}, f32[64,256]{1,0:T(8,128)}, f32[64,512]{1,0:T(8,128)}, f32[8,256]{1,0:T(8,128)}, /*index=...) custom-call(f32[64,256]{1,0:T(8,128)S(1)} %get-tuple-element.30.refs, ...), custom_call_target="tpu_custom_call" | custom-call | tf_op jit(solution)/shard_map/pallas_call | solution.py:471

commit v3 on v2

--- a/solution.py
+++ b/solution.py
@@ -119,10 +119,15 @@
 MESH = pl.DeviceIdType.MESH
 VMEM_LIMIT = 60 * 2**20
 OUT_LIMIT = 16 * 2**20
-CHUNKS = (0, 1)
-EARLY_Z = (1, 2)
+CHUNKS = (1, 0)
+EARLY_Z = (2,)
+PIECES = 2
+FINAL = ('G0', 'G1', 'F0', 'F1', 'S0', 'S1', 'N1', '10', 'N0', '20', '11', '21', '30', '31')
 OFF_Z = True
-PLAN = {'sent': (('z', 2, 0), ('z', 1, 1)), 'second0': (('r', 0, 0), ('r', 1, 0)), 'second1': (('r', 0, 1), ('r', 1, 1)), 'fourth1': (('z', 1, 0), ('z', 2, 1))}
+YIELD = 2
+DIAG = ((0, 3),)
+RELAY = {'third0': 1}
+PLAN = {'second1': (('r', 0, 1, 1, None), ('r', 1, 1, 1, None), ('r', 0, 0, 1, None), ('r', 1, 0, 1, None)), 'recv12': (('z', 2, 1, 1, None),), 'recv10': (('r', 1, 1, 0, None), ('r', 0, 1, 0, None)), 'sent': (('z', 2, 0, 1, None), ('z', 2, 0, 0, None)), 'fourth0': (('z', 2, 1, 0, None),), 'third0': (('r', 0, 0, 0, None), ('r', 1, 0, 0, None))}
 f32, bf16 = jnp.float32, jnp.bfloat16
 
 
@@ -196,38 +201,67 @@
         ("first", 0): (qf_hbm, qf), ("first", 1): (vf_hbm, vf),
         ("second", 0): (qs_hbm, qs), ("second", 1): (vs_hbm, vs),
     }
-    names = ["x"] + [(n, c) for c in CHUNKS for n in ("basis", "cot")]
-    names += [(n, c) for n in ("weight", "first", "second") for c in CHUNKS]
-    loads = {
-        n: pltpu.make_async_copy(sources[n][0], sources[n][1], load.at[i])
-        for i, n in enumerate(names)
-    }
-    for c in loads.values():
-        c.start()
-
-    early = {}
+    c0, c1 = CHUNKS
+    groups = [
+        ["x", ("basis", c0)],
+        [("cot", c0)],
+        [("basis", c1), ("cot", c1)],
+        [("weight", c0), ("weight", c1)],
+        [(n, c) for n in ("first", "second") for c in CHUNKS],
+    ]
+    for i, group in enumerate(groups):
+        for n in group:
+            pltpu.make_async_copy(*sources[n], load.at[i]).start()
+
+    def loaded(i):
+        settle(spare.at[: sum(size_of(sources[n][1]) for n in groups[i]) // 512], load.at[i])
 
     def run(point):
-        for kind, k, c in PLAN.get(point, ()):
-            if ("weight", c) in loads:
-                loads.pop(("weight", c)).wait()
+        if point in RELAY:
+            c = CHUNKS[RELAY[point]]
+            settle(z_weight[c].at[0], in8.at[c, 1])
+            remote(z_weight[c].at[1], z_weight[c].at[2], in8.at[c, 2], {"fs": zs[1]})
+        for core in (None, 0, 1):
+            pieces = [q[:4] for q in PLAN.get(point, ()) if q[4] == core]
+            if pieces:
+                by_core(core, functools.partial(send_pieces, pieces))
+
+    def send_pieces(pieces):
+        for kind, k, c, p in pieces:
+            part_rows = pl.ds(p * (rows // PIECES), rows // PIECES)
+            source = weight[c].at[part_rows]
             if kind == "z":
-                d = remote(weight[c], z_weight[c].at[k - 1], in8.at[c, k - 1], {"fs": zs[k]})
+                remote(source, z_weight[c].at[k - 1, part_rows], in8.at[c, k - 1], {"fs": zs[k]})
             else:
-                d = remote(weight[c], r_weight[c].at[k], in9.at[c, k], {"rep": rs[k + 1]})
-            early[kind, k, c] = d
+                remote(source, r_weight[c].at[k, part_rows], in9.at[c, k], {"rep": rs[k + 1]})
+
+    def by_core(core, body):
+        if core is None:
+            return body()
+        scope(None)
+        n, m = len(total_sent), len(total_rest)
+        pl.when(t == core)(body)
+        if core > 0:
+            del total_sent[n:]
+            del total_rest[m:]
 
     far = (2, 3, 1, 0)
+
+    def send_first(c):
+        for j in far:
+            for k in range(1, R):
+                remote(part[c].at[rs[k], zs[j]], got1[c].at[k, j], in1.at[c, j], {"rep": rs[k]})
+
     for i, c in enumerate(CHUNKS):
         scope(f"p01_load_dot#c={c}")
+        loaded(2 * i)
         if i == 0:
-            loads.pop("x").wait()
             x = x_ref[...]
-        loads.pop(("basis", c)).wait()
         reduced = jnp.dot(x, basis[c][...], preferred_element_type=f32).T
         high, low = two_parts(reduced)
         both = jnp.concatenate([high, low], axis=1)
-        loads.pop(("cot", c)).wait()
+        if i == 0:
+            loaded(1)
         g = cot[c][...]
         total = jnp.dot(both, jnp.concatenate([g, g], axis=0), preferred_element_type=f32)
         for a in range(F):
@@ -238,15 +272,16 @@
             scope("p02_barrier")
             pl.semaphore_wait(barrier, F + R + T - 3)
         scope(f"p03_send1#c={c}")
-        for j in far:
-            for k in range(1, R):
-                remote(part[c].at[rs[k], zs[j]], got1[c].at[k, j], in1.at[c, j], {"rep": rs[k]})
+        by_core(0 if i and YIELD else None, functools.partial(send_first, c))
+    loaded(3)
     run("sent")
 
     own = {}
     for c in CHUNKS:
         scope(f"p04_recv1#c={c}")
-        for j in far:
+        for n, j in enumerate(far):
+            if YIELD and c == CHUNKS[0] and n == YIELD - 1:
+                by_core(1, functools.partial(send_first, CHUNKS[1]))
             total = part[c][r, zs[j]]
             settle(got1[c].at[1:R, j], in1.at[c, j])
             for k in range(1, R):
@@ -256,7 +291,8 @@
                 remote(mid[c].at[j], got2[c].at[j], in2.at[c], {"fs": zs[j]})
             else:
                 own[c] = total
-        run(f"second{c}")
+            run(f"recv{CHUNKS.index(c)}{n}")
+        run(f"second{CHUNKS.index(c)}")
 
     third, sums = {}, []
 
@@ -267,8 +303,8 @@
 
     for c in CHUNKS:
         scope(f"p05_recv2#c={c}")
-        loads.pop(("first", c)).wait()
-        loads.pop(("second", c)).wait()
+        if c == c0:
+            loaded(4)
         projected = own[c]
         settle(got2[c].at[1:F], in2.at[c])
         for j in (1, 3, 2):
@@ -295,14 +331,15 @@
         spread(c, 0)
         first_out[c][...] = fn
         second_out[c][...] = sn
-        run(f"third{c}")
+        run(f"third{CHUNKS.index(c)}")
 
     for c in CHUNKS:
         scope(f"p06_recv3#c={c}")
-        for j in (1, 3, 2):
+        for n, j in enumerate((1, 3, 2)):
             third[c, j].wait_recv()
             spread(c, j)
-        run(f"fourth{c}")
+            run(f"spread{CHUNKS.index(c)}{n}")
+        run(f"fourth{CHUNKS.index(c)}")
 
     def start_of(j, k):
         return pl.multiple_of((zs[j] * R + rs[k]) * rows, rows)
@@ -324,90 +361,111 @@
         remote(block, block, rest.at[0], {"rep": rs[2 - a]}, True)
 
     def send_direct(c, j, order=((0, 0), (1, 1), (0, 1), (1, 0))):
+        if (CHUNKS.index(c), j) in DIAG:
+            block = copy[c].at[pl.ds(start_of(j, 0), rows), :]
+            for k in (3, 1, 2):
+                remote(block, block, rest.at[0], {"rep": rs[k]}, True)
+            return
         for a, p in order:
             block = piece(c, j, 0, p)
             if a == p:
-                direct[c, j, a] = remote(block, block, in7.at[c, j - 1, a], {"rep": rs[a + 1]})
+                direct[c, j, a] = remote(block, block, in7.at[c, j - 2, a], {"rep": rs[a + 1]})
             else:
                 remote(block, block, rest.at[0], {"rep": rs[a + 1]}, True)
 
-    late = [j for j in range(1, F) if j not in EARLY_Z]
-    waiting = []
-    for c in CHUNKS:
+    late = [j for j in range(1, F) if j not in EARLY_Z and not (OFF_Z and j == 1)]
+    waiting, sq = [], None
+
+    def gather(c):
+        nonlocal sq
         scope(f"p07_recv4#c={c}")
         settle(dirs[c].at[:, 1:R], in4.at[c])
         scope(f"p08_square#c={c}")
         whole = dirs[c][...].reshape(F * R * M, width[c])
         dd = jnp.concatenate(two_parts(whole), axis=0)
-        blocks = [(0, 0), (1, 0), (0, 1), (0, 2)] + [(j, 0) for j in EARLY_Z if j > 1]
-        raw = product(c, dd, blocks[:4])
-        raw_far = product(c, dd, blocks[4:]) if blocks[4:] else None
+        relayed = CHUNKS.index(c) in RELAY.values()
+        blocks = [(0, 0), (0, 1), (0, 2), (2, 0)] + ([(3, 0)] if relayed else [])
+        raw = product(c, dd, blocks[:3])
+        raw_far = product(c, dd, blocks[3:]) if blocks[3:] else None
         scope(f"p09_fifth#c={c}")
         if c == CHUNKS[0]:
             settle(spare.at[: F * R * T - 1], in5.at[0])
             sq = jnp.sum(norms[...].reshape(F * R * T, 128), axis=0, keepdims=True)
         count = F * R * M * width[c] * T
         inverse = 1.0 / jnp.sqrt(sq[:, 64 * c : 64 * c + 1] / count + 1.0)
-        if ("weight", c) in loads:
-            loads.pop(("weight", c)).wait()
         scope(f"p10_copy#c={c}")
         for n, (j, k) in enumerate(blocks):
-            source = raw if n < 4 else raw_far
-            update = source[n % 4 * rows : (n % 4 + 1) * rows] * inverse
+            source = raw if n < 3 else raw_far
+            at = n if n < 3 else n - 3
+            update = source[at * rows : (at + 1) * rows] * inverse
             if n == 0:
                 new = weight[c][...] - 0.01 * update
                 update_out[c][...] = update
                 weight_out[c][...] = new
             elif k == 0:
-                if j > 1:
-                    waiting.append((c, j, update))
-                    continue
-                early["z", j, c].wait_recv()
-                new = z_weight[c][j - 1] - 0.01 * update
+                waiting.append((c, j, update))
+                continue
             else:
-                early["r", k - 1, c].wait_recv()
+                settle(r_weight[c].at[0], in9.at[c, k - 1])
                 new = r_weight[c][k - 1] - 0.01 * update
             copy[c][pl.ds(start_of(j, k), rows), :] = new.astype(bf16)
-            if n == 0:
-                for j2 in late:
-                    block = copy[c].at[pl.ds(start_of(0, 0), rows), :]
-                    sixth[c, j2] = remote(block, block, in6.at[c, j2 - 1], {"fs": zs[j2]})
-            elif k == 0 and not OFF_Z:
-                send_direct(c, j)
-            elif k > 0 and OFF_Z:
+            if k > 0 and OFF_Z:
                 block = piece(c, 0, k, k - 1)
                 across[c, k - 1] = remote(block, block, in10.at[c, k - 1], {"fs": zs[1]})
-                block = piece(c, 0, k, 2 - k)
-                remote(block, block, rest.at[0], {"fs": zs[1]}, True)
         for a in range(2):
             pass_on(c, 0, a)
-        run(f"final{c}")
-    for c, j, update in waiting:
-        scope(f"p115_far#c={c}")
-        early["z", j, c].wait_recv()
-        new = z_weight[c][j - 1] - 0.01 * update
-        copy[c][pl.ds(start_of(j, 0), rows), :] = new.astype(bf16)
-        send_direct(c, j)
-
-    for c in CHUNKS:
+
+    def others(c):
+        for k in (1, 2):
+            block = piece(c, 0, k, 2 - k)
+            remote(block, block, rest.at[0], {"fs": zs[1]}, True)
+        block = copy[c].at[pl.ds(start_of(0, 0), rows), :]
+        remote(block, block, rest.at[0], {"fs": zs[1]}, True)
+
+    def far_rows(c):
+        for owner, j, update in waiting:
+            if owner == c:
+                scope(f"p115_far#c={c}")
+                relayed = CHUNKS.index(c) in RELAY.values()
+                if not relayed or j == 3:
+                    settle(z_weight[c].at[0], in8.at[c, j - 1])
+                new = z_weight[c][j - 1] - 0.01 * update
+                copy[c][pl.ds(start_of(j, 0), rows), :] = new.astype(bf16)
+                if not relayed:
+                    block = copy[c].at[pl.ds(start_of(j, 0), rows), :]
+                    sixth[c, 3] = remote(block, block, in6.at[c, 0], {"fs": zs[1]})
+                send_direct(c, j)
+
+    def sixth_rows(c):
+        if CHUNKS.index(c) in RELAY.values():
+            return
         scope(f"p12_sixth#c={c}")
         for j in late:
             sixth[c, j].wait_recv()
             send_direct(c, j)
-    for c in CHUNKS:
-        for j in range(1, F):
-            if j in late:
-                continue
-            scope(f"p13_pass#c={c}#j={j}")
-            for a in range(2):
-                (across[c, a] if OFF_Z and j == 1 else direct[c, j, a]).wait_recv()
-                pass_on(c, j, a)
-    for c in CHUNKS:
-        for j in late:
-            scope(f"p14_pass#c={c}#j={j}")
-            for a in range(2):
-                direct[c, j, a].wait_recv()
-                pass_on(c, j, a)
+
+    def pass_rows(c, j):
+        if (CHUNKS.index(c), j) in DIAG:
+            return
+        scope(f"p13_pass#c={c}#j={j}")
+        for a in range(2):
+            (across[c, a] if OFF_Z and j == 1 else direct[c, j, a]).wait_recv()
+            pass_on(c, j, a)
+
+    for step in FINAL:
+        c = CHUNKS[int(step[1])]
+        if step[0] == "N":
+            others(c)
+        elif step[0] == "G":
+            gather(c)
+        elif step[0] in "OP":
+            by_core(0 if step[0] == "O" else 1, functools.partial(others, c))
+        elif step[0] == "F":
+            far_rows(c)
+        elif step[0] == "S":
+            sixth_rows(c)
+        else:
+            pass_rows(c, int(step[0]))
     scope("p15_last")
     settle(spare.at[: sum(total_rest) // 512], rest.at[0])
     scope("p16_waitsend")
@@ -416,15 +474,12 @@
 
 
 def write_out(*refs):
-    sem, sources, targets = refs[20], refs[:10], refs[10:20]
-    copies = [
-        pltpu.make_async_copy(src, dst, sem.at[i])
-        for i, (src, dst) in enumerate(zip(sources, targets))
-    ]
+    sem, sources, targets = refs[-1].at[0], refs[:10], refs[10:20]
+    copies = [pltpu.make_async_copy(src, dst, sem) for src, dst in zip(sources, targets)]
     for c in copies[::-1]:
         c.start()
-    for c in copies[::-1]:
-        c.wait()
+    whole = refs[-2].at[: sum(size_of(src) for src in sources) // 512]
+    pltpu.make_async_copy(whole, whole, sem).wait()
 
 
 def fused(plain, *args):
@@ -444,7 +499,7 @@
         return [pltpu.VMEM(shape + (w,), dtype) for w in W]
 
     sems = [
-        (11,), (1,), (2, F), (2,), (2, F - 1), (2,), (1,), (2, F - 1), (2, F - 1, 2), (2, F - 1), (2, 2), (2, 2), (1,),
+        (5,), (1,), (2, F), (2,), (2, F - 1), (2,), (1,), (2, 1), (2, 2, 2), (2, F - 1), (2, 2), (2, 2), (1,),
     ]
     results = pl.pallas_call(
         functools.partial(kernel, T),
@@ -477,7 +532,7 @@
         ],
         in_specs=[vmem] * 10,
         out_specs=[pl.BlockSpec(memory_space=pltpu.HBM)] * 10,
-        scratch_shapes=[dma((10,))],
+        scratch_shapes=[pltpu.VMEM((8 * rows * F * R, 128), f32), dma((1,))],
         compiler_params=pltpu.CompilerParams(vmem_limit_bytes=OUT_LIMIT),
     )(*results)
     qu, vu, qn, vn, qfn, vfn, qsn, vsn, qcopy, vcopy = outs

time: 37.2 us -> 34.8 us (0.935)
  Pallas kernels: 36.4 us -> 34 us
    pallas_call x1, Pallas kernels: 35 us -> 32.7 us  [fused(): pl.pallas_call(functools.partial(kernel, T), out_shape=each(rows) + each(...]
where the time goes in v3:
time: 34.8 us; the launch traced here: 34.7 us
  Pallas kernels  34 us (98%)
  between operations  0.65 us (2%)
    pallas_call x1, Pallas kernels, fused(): pl.pallas_call(functools.partial(kernel, T), out_shape=each(rows) + each(...  32.7 us
    pallas_call x1, Pallas kernels, fused(): pl.pallas_call(write_out, out_shape=[out(qw.shape, f32), out(vw.shape, f3...  1.29 us

profile of v3, /device:TPU:0, one launch (start us, length us, event | category | flops | bytes accessed | tf_op | source)
XLA Modules:
  0.0 34.7 jit_solution(8734677382580099258)
XLA Ops:
  0.6 32.7 %shard_map.186 = (f32[64,256]{1,0:T(8,128)S(1)}, f32[64,512]{1,0:T(8,128)S(1)}, f32[64,256]{1,0:T(8,128)S(1)}, f32[64,512]{1,0:T(8,128)S(1)}, f32[8,256]{1,0:T(8...) custom-call(bf16[128,1024]{1,0:T(8,128)(2,1)} %x_hbm.1, ...), custom_call_target="tpu_custom_call" | custom-call | tf_op jit(solution)/shard_map/pallas_call | solution.py:504
  33.4 1.3 %shard_map.187 = (f32[64,256]{1,0:T(8,128)}, f32[64,512]{1,0:T(8,128)}, f32[64,256]{1,0:T(8,128)}, f32[64,512]{1,0:T(8,128)}, f32[8,256]{1,0:T(8,128)}, /*index=...) custom-call(f32[64,256]{1,0:T(8,128)S(1)} %get-tuple-element.30.refs, ...), custom_call_target="tpu_custom_call" | custom-call | tf_op jit(solution)/shard_map/pallas_call | solution.py:526

commit v4 on v3

--- a/solution.py
+++ b/solution.py
@@ -120,19 +120,13 @@
 VMEM_LIMIT = 60 * 2**20
 OUT_LIMIT = 16 * 2**20
 CHUNKS = (1, 0)
-EARLY_Z = (2,)
 PIECES = 2
-FINAL = ('G0', 'G1', 'F0', 'F1', 'S0', 'S1', 'N1', '10', 'N0', '20', '11', '21', '30', '31')
-OFF_Z = True
+FINAL = ('G0', 'G1', 'F0', 'F1', 'O1', 'S1', 'O0', 'P1', 'S0', '10', '21', 'P0', '20', '11', '31', '30')
 YIELD = 2
-DIAG = ((0, 3),)
-RELAY = {'third0': 1}
-PLAN = {'second1': (('r', 0, 1, 1, None), ('r', 1, 1, 1, None), ('r', 0, 0, 1, None), ('r', 1, 0, 1, None)), 'recv12': (('z', 2, 1, 1, None),), 'recv10': (('r', 1, 1, 0, None), ('r', 0, 1, 0, None)), 'sent': (('z', 2, 0, 1, None), ('z', 2, 0, 0, None)), 'fourth0': (('z', 2, 1, 0, None),), 'third0': (('r', 0, 0, 0, None), ('r', 1, 0, 0, None))}
+DIAG = ((0, 3), (1, 3))
+RELAY = {'third1': 1}
+PLAN = {'sent': (('z', 2, 0, 1, None), ('z', 2, 1, 1, 1), ('z', 2, 0, 0, None)), 'recv11': (('z', 2, 1, 1, 0), ('r', 0, 0, 0, None), ('r', 1, 0, 0, None)), 'second1': (('r', 0, 1, 1, None), ('r', 1, 1, 1, None), ('r', 1, 0, 1, None), ('r', 0, 0, 1, None)), 'recv10': (('r', 1, 1, 0, None), ('r', 0, 1, 0, None)), 'fourth0': (('z', 2, 1, 0, None),)}
 f32, bf16 = jnp.float32, jnp.bfloat16
-
-
-def scope(name):
-    pass
 
 
 def two_parts(x):
@@ -188,7 +182,6 @@
     def settle(ref, sem):
         pltpu.make_async_copy(ref, ref, sem).wait()
 
-    scope("p00_sig_load")
     barrier = pltpu.get_barrier_semaphore()
     for axis, others in (("rep", rs), ("fs", zs), ("tp", ts)):
         for other in others[1:]:
@@ -219,8 +212,8 @@
     def run(point):
         if point in RELAY:
             c = CHUNKS[RELAY[point]]
-            settle(z_weight[c].at[0], in8.at[c, 1])
-            remote(z_weight[c].at[1], z_weight[c].at[2], in8.at[c, 2], {"fs": zs[1]})
+            settle(z_weight[c].at[0], in8.at[c, 0])
+            remote(z_weight[c].at[1], z_weight[c].at[2], in8.at[c, 1], {"fs": zs[1]})
         for core in (None, 0, 1):
             pieces = [q[:4] for q in PLAN.get(point, ()) if q[4] == core]
             if pieces:
@@ -231,14 +224,13 @@
             part_rows = pl.ds(p * (rows // PIECES), rows // PIECES)
             source = weight[c].at[part_rows]
             if kind == "z":
-                remote(source, z_weight[c].at[k - 1, part_rows], in8.at[c, k - 1], {"fs": zs[k]})
+                remote(source, z_weight[c].at[k - 1, part_rows], in8.at[c, k - 2], {"fs": zs[k]})
             else:
-                remote(source, r_weight[c].at[k, part_rows], in9.at[c, k], {"rep": rs[k + 1]})
+                remote(source, r_weight[c].at[k, part_rows], in9.at[c], {"rep": rs[k + 1]})
 
     def by_core(core, body):
         if core is None:
             return body()
-        scope(None)
         n, m = len(total_sent), len(total_rest)
         pl.when(t == core)(body)
         if core > 0:
@@ -253,7 +245,6 @@
                 remote(part[c].at[rs[k], zs[j]], got1[c].at[k, j], in1.at[c, j], {"rep": rs[k]})
 
     for i, c in enumerate(CHUNKS):
-        scope(f"p01_load_dot#c={c}")
         loaded(2 * i)
         if i == 0:
             x = x_ref[...]
@@ -269,16 +260,13 @@
                 at = (a * R + b) * M
                 part[c][b, a] = total[at : at + M]
         if i == 0:
-            scope("p02_barrier")
             pl.semaphore_wait(barrier, F + R + T - 3)
-        scope(f"p03_send1#c={c}")
         by_core(0 if i and YIELD else None, functools.partial(send_first, c))
     loaded(3)
     run("sent")
 
     own = {}
     for c in CHUNKS:
-        scope(f"p04_recv1#c={c}")
         for n, j in enumerate(far):
             if YIELD and c == CHUNKS[0] and n == YIELD - 1:
                 by_core(1, functools.partial(send_first, CHUNKS[1]))
@@ -302,7 +290,6 @@
             remote(block, block, in4.at[c], {"rep": rs[k]})
 
     for c in CHUNKS:
-        scope(f"p05_recv2#c={c}")
         if c == c0:
             loaded(4)
         projected = own[c]
@@ -314,7 +301,6 @@
         dirs[c][z, r] = fn / (jnp.sqrt(sn) + 1e-08)
         sums.append(jnp.sum(dirs[c][z, r] * dirs[c][z, r], keepdims=True))
         if c == CHUNKS[-1]:
-            scope("p055_norms")
             lane = lax.broadcasted_iota(jnp.int32, (1, 128), 1)
             slot = (z * R + r) * T + t
             norms[slot] = jnp.where(lane < 64, sums[CHUNKS.index(0)], sums[CHUNKS.index(1)])
@@ -324,7 +310,6 @@
                         if j or k or n:
                             peer = {"fs": zs[j], "rep": rs[k], "tp": ts[n]}
                             remote(norms.at[slot], norms.at[slot], in5.at[0], peer)
-            scope(f"p056_third#c={c}")
         block = dirs[c].at[z, r]
         for j in (2, 3, 1):
             third[c, j] = remote(block, block, in3.at[c, j - 1], {"fs": zs[j]})
@@ -334,7 +319,6 @@
         run(f"third{CHUNKS.index(c)}")
 
     for c in CHUNKS:
-        scope(f"p06_recv3#c={c}")
         for n, j in enumerate((1, 3, 2)):
             third[c, j].wait_recv()
             spread(c, j)
@@ -373,27 +357,22 @@
             else:
                 remote(block, block, rest.at[0], {"rep": rs[a + 1]}, True)
 
-    late = [j for j in range(1, F) if j not in EARLY_Z and not (OFF_Z and j == 1)]
     waiting, sq = [], None
 
     def gather(c):
         nonlocal sq
-        scope(f"p07_recv4#c={c}")
         settle(dirs[c].at[:, 1:R], in4.at[c])
-        scope(f"p08_square#c={c}")
         whole = dirs[c][...].reshape(F * R * M, width[c])
         dd = jnp.concatenate(two_parts(whole), axis=0)
         relayed = CHUNKS.index(c) in RELAY.values()
         blocks = [(0, 0), (0, 1), (0, 2), (2, 0)] + ([(3, 0)] if relayed else [])
         raw = product(c, dd, blocks[:3])
         raw_far = product(c, dd, blocks[3:]) if blocks[3:] else None
-        scope(f"p09_fifth#c={c}")
         if c == CHUNKS[0]:
             settle(spare.at[: F * R * T - 1], in5.at[0])
             sq = jnp.sum(norms[...].reshape(F * R * T, 128), axis=0, keepdims=True)
         count = F * R * M * width[c] * T
         inverse = 1.0 / jnp.sqrt(sq[:, 64 * c : 64 * c + 1] / count + 1.0)
-        scope(f"p10_copy#c={c}")
         for n, (j, k) in enumerate(blocks):
             source = raw if n < 3 else raw_far
             at = n if n < 3 else n - 3
@@ -406,10 +385,11 @@
                 waiting.append((c, j, update))
                 continue
             else:
-                settle(r_weight[c].at[0], in9.at[c, k - 1])
+                if k == 1:
+                    settle(r_weight[c], in9.at[c])
                 new = r_weight[c][k - 1] - 0.01 * update
             copy[c][pl.ds(start_of(j, k), rows), :] = new.astype(bf16)
-            if k > 0 and OFF_Z:
+            if k > 0:
                 block = piece(c, 0, k, k - 1)
                 across[c, k - 1] = remote(block, block, in10.at[c, k - 1], {"fs": zs[1]})
         for a in range(2):
@@ -425,10 +405,9 @@
     def far_rows(c):
         for owner, j, update in waiting:
             if owner == c:
-                scope(f"p115_far#c={c}")
                 relayed = CHUNKS.index(c) in RELAY.values()
                 if not relayed or j == 3:
-                    settle(z_weight[c].at[0], in8.at[c, j - 1])
+                    settle(z_weight[c].at[0], in8.at[c, j - 2])
                 new = z_weight[c][j - 1] - 0.01 * update
                 copy[c][pl.ds(start_of(j, 0), rows), :] = new.astype(bf16)
                 if not relayed:
@@ -439,17 +418,14 @@
     def sixth_rows(c):
         if CHUNKS.index(c) in RELAY.values():
             return
-        scope(f"p12_sixth#c={c}")
-        for j in late:
-            sixth[c, j].wait_recv()
-            send_direct(c, j)
+        sixth[c, 3].wait_recv()
+        send_direct(c, 3)
 
     def pass_rows(c, j):
         if (CHUNKS.index(c), j) in DIAG:
             return
-        scope(f"p13_pass#c={c}#j={j}")
         for a in range(2):
-            (across[c, a] if OFF_Z and j == 1 else direct[c, j, a]).wait_recv()
+            (across[c, a] if j == 1 else direct[c, j, a]).wait_recv()
             pass_on(c, j, a)
 
     for step in FINAL:
@@ -466,11 +442,8 @@
             sixth_rows(c)
         else:
             pass_rows(c, int(step[0]))
-    scope("p15_last")
     settle(spare.at[: sum(total_rest) // 512], rest.at[0])
-    scope("p16_waitsend")
     settle(spare.at[: sum(total_sent) // 512], sent.at[0])
-    scope(None)
 
 
 def write_out(*refs):
@@ -499,7 +472,7 @@
         return [pltpu.VMEM(shape + (w,), dtype) for w in W]
 
     sems = [
-        (5,), (1,), (2, F), (2,), (2, F - 1), (2,), (1,), (2, 1), (2, 2, 2), (2, F - 1), (2, 2), (2, 2), (1,),
+        (5,), (1,), (2, F), (2,), (2, F - 1), (2,), (1,), (2, 1), (2, 2, 2), (2, 2), (2,), (2, 2), (1,),
     ]
     results = pl.pallas_call(
         functools.partial(kernel, T),

time: 34.8 us -> 34.7 us (level)
  no operation moved by 1% of the time
where the time goes in v4:
time: 34.7 us; the launch traced here: 34.5 us
  Pallas kernels  33.9 us (98%)
  between operations  0.65 us (2%)
    pallas_call x1, Pallas kernels, fused(): pl.pallas_call(functools.partial(kernel, T), out_shape=each(rows) + each(...  32.6 us
    pallas_call x1, Pallas kernels, fused(): pl.pallas_call(write_out, out_shape=[out(qw.shape, f32), out(vw.shape, f3...  1.29 us

profile of v4, /device:TPU:0, one launch (start us, length us, event | category | flops | bytes accessed | tf_op | source)
XLA Modules:
  0.0 34.5 jit_solution(13698582823056349488)
XLA Ops:
  0.6 32.6 %shard_map.186 = (f32[64,256]{1,0:T(8,128)S(1)}, f32[64,512]{1,0:T(8,128)S(1)}, f32[64,256]{1,0:T(8,128)S(1)}, f32[64,512]{1,0:T(8,128)S(1)}, f32[8,256]{1,0:T(8...) custom-call(bf16[128,1024]{1,0:T(8,128)(2,1)} %x_hbm.1, ...), custom_call_target="tpu_custom_call" | custom-call | tf_op jit(solution)/shard_map/pallas_call | solution.py:477
  33.2 1.3 %shard_map.187 = (f32[64,256]{1,0:T(8,128)}, f32[64,512]{1,0:T(8,128)}, f32[64,256]{1,0:T(8,128)}, f32[64,512]{1,0:T(8,128)}, f32[8,256]{1,0:T(8,128)}, /*index=...) custom-call(f32[64,256]{1,0:T(8,128)S(1)} %get-tuple-element.30.refs, ...), custom_call_target="tpu_custom_call" | custom-call | tf_op jit(solution)/shard_map/pallas_call | solution.py:499

commit v5 on v4

--- a/solution.py
+++ b/solution.py
@@ -300,6 +300,10 @@
         sn = 0.99 * second[c][...] + 0.01 * projected * projected
         dirs[c][z, r] = fn / (jnp.sqrt(sn) + 1e-08)
         sums.append(jnp.sum(dirs[c][z, r] * dirs[c][z, r], keepdims=True))
+        block = dirs[c].at[z, r]
+        for j in (2, 3, 1):
+            third[c, j] = remote(block, block, in3.at[c, j - 1], {"fs": zs[j]})
+        spread(c, 0)
         if c == CHUNKS[-1]:
             lane = lax.broadcasted_iota(jnp.int32, (1, 128), 1)
             slot = (z * R + r) * T + t
@@ -310,10 +314,6 @@
                         if j or k or n:
                             peer = {"fs": zs[j], "rep": rs[k], "tp": ts[n]}
                             remote(norms.at[slot], norms.at[slot], in5.at[0], peer)
-        block = dirs[c].at[z, r]
-        for j in (2, 3, 1):
-            third[c, j] = remote(block, block, in3.at[c, j - 1], {"fs": zs[j]})
-        spread(c, 0)
         first_out[c][...] = fn
         second_out[c][...] = sn
         run(f"third{CHUNKS.index(c)}")

time: 34.7 us -> 34.5 us (level)
  no operation moved by 1% of the time
where the time goes in v5:
time: 34.5 us; the launch traced here: 34.3 us
  Pallas kernels  33.7 us (98%)
  between operations  0.65 us (2%)
    pallas_call x1, Pallas kernels, fused(): pl.pallas_call(functools.partial(kernel, T), out_shape=each(rows) + each(...  32.4 us
    pallas_call x1, Pallas kernels, fused(): pl.pallas_call(write_out, out_shape=[out(qw.shape, f32), out(vw.shape, f3...  1.29 us

profile of v5, /device:TPU:0, one launch (start us, length us, event | category | flops | bytes accessed | tf_op | source)
XLA Modules:
  0.0 34.3 jit_solution(17992922671368422957)
XLA Ops:
  0.6 32.4 %shard_map.186 = (f32[64,256]{1,0:T(8,128)S(1)}, f32[64,512]{1,0:T(8,128)S(1)}, f32[64,256]{1,0:T(8,128)S(1)}, f32[64,512]{1,0:T(8,128)S(1)}, f32[8,256]{1,0:T(8...) custom-call(bf16[128,1024]{1,0:T(8,128)(2,1)} %x_hbm.1, ...), custom_call_target="tpu_custom_call" | custom-call | tf_op jit(solution)/shard_map/pallas_call | solution.py:477
  33.1 1.3 %shard_map.187 = (f32[64,256]{1,0:T(8,128)}, f32[64,512]{1,0:T(8,128)}, f32[64,256]{1,0:T(8,128)}, f32[64,512]{1,0:T(8,128)}, f32[8,256]{1,0:T(8,128)}, /*index=...) custom-call(f32[64,256]{1,0:T(8,128)S(1)} %get-tuple-element.30.refs, ...), custom_call_target="tpu_custom_call" | custom-call | tf_op jit(solution)/shard_map/pallas_call | solution.py:499

commit v6 on v5

--- a/solution.py
+++ b/solution.py
@@ -353,7 +353,7 @@
         for a, p in order:
             block = piece(c, j, 0, p)
             if a == p:
-                direct[c, j, a] = remote(block, block, in7.at[c, j - 2, a], {"rep": rs[a + 1]})
+                direct[c, j, a] = remote(block, block, in7.at[c, a], {"rep": rs[a + 1]})
             else:
                 remote(block, block, rest.at[0], {"rep": rs[a + 1]}, True)
 
@@ -412,7 +412,7 @@
                 copy[c][pl.ds(start_of(j, 0), rows), :] = new.astype(bf16)
                 if not relayed:
                     block = copy[c].at[pl.ds(start_of(j, 0), rows), :]
-                    sixth[c, 3] = remote(block, block, in6.at[c, 0], {"fs": zs[1]})
+                    sixth[c, 3] = remote(block, block, in6.at[0], {"fs": zs[1]})
                 send_direct(c, j)
 
     def sixth_rows(c):
@@ -472,7 +472,7 @@
         return [pltpu.VMEM(shape + (w,), dtype) for w in W]
 
     sems = [
-        (5,), (1,), (2, F), (2,), (2, F - 1), (2,), (1,), (2, 1), (2, 2, 2), (2, 2), (2,), (2, 2), (1,),
+        (5,), (1,), (2, F), (2,), (2, F - 1), (2,), (1,), (1,), (2, 2), (2, 2), (2,), (2, 2), (1,),
     ]
     results = pl.pallas_call(
         functools.partial(kernel, T),

time: 34.5 us -> 34.5 us (level)
  no operation moved by 1% of the time
where the time goes in v6:
time: 34.5 us; the launch traced here: 34.3 us
  Pallas kernels  33.6 us (97%)
  between operations  0.65 us (2%)
    pallas_call x1, Pallas kernels, fused(): pl.pallas_call(functools.partial(kernel, T), out_shape=each(rows) + each(...  32.4 us
    pallas_call x1, Pallas kernels, fused(): pl.pallas_call(write_out, out_shape=[out(qw.shape, f32), out(vw.shape, f3...  1.29 us

profile of v6, /device:TPU:0, one launch (start us, length us, event | category | flops | bytes accessed | tf_op | source)
XLA Modules:
  0.0 34.3 jit_solution(12176395685406916653)
XLA Ops:
  0.6 32.4 %shard_map.186 = (f32[64,256]{1,0:T(8,128)S(1)}, f32[64,512]{1,0:T(8,128)S(1)}, f32[64,256]{1,0:T(8,128)S(1)}, f32[64,512]{1,0:T(8,128)S(1)}, f32[8,256]{1,0:T(8...) custom-call(bf16[128,1024]{1,0:T(8,128)(2,1)} %x_hbm.1, ...), custom_call_target="tpu_custom_call" | custom-call | tf_op jit(solution)/shard_map/pallas_call | solution.py:477
  33.0 1.3 %shard_map.187 = (f32[64,256]{1,0:T(8,128)}, f32[64,512]{1,0:T(8,128)}, f32[64,256]{1,0:T(8,128)}, f32[64,512]{1,0:T(8,128)}, f32[8,256]{1,0:T(8,128)}, /*index=...) custom-call(f32[64,256]{1,0:T(8,128)S(1)} %get-tuple-element.30.refs, ...), custom_call_target="tpu_custom_call" | custom-call | tf_op jit(solution)/shard_map/pallas_call | solution.py:499
